TPU v7x, 128 devices: a whole 4x4x4 slice. The times are simulated.
128 devices in a mesh: sp: 16 (over z, y), dp: 8 (over x, core).
Axes of the slice: x: 4, y: 4, z: 4, core: 2. Of those that a mesh axis runs over, the one named last changes fastest.
Arguments:
- u_pre: bfloat16 [8, 16384, 2048], P('dp', 'sp'), may hold values from -6 to 6
- v_pre: bfloat16 [8, 16384, 2048], P('dp', 'sp'), may hold values from -6 to 6
- d_out: bfloat16 [8, 16384, 2048], P('dp', 'sp'), may hold values from -6 to 6
- w_mix: bfloat16 [16, 128, 128], replicated, may hold values from -0.5 to 0.5
- mix_bias: float32 [16, 128], replicated, may hold values from 0.1 to 1.9
- norm_gain: float32 [16, 128], replicated, may hold values from 0.1 to 1.9
- norm_shift: float32 [16, 128], replicated, may hold values from -3 to 3
- w_out: bfloat16 [2048, 2048], P('dp'), may hold values from -0.125 to 0.125
Outputs:
- grad_u: bfloat16 [8, 16384, 2048], P('dp', 'sp')
- grad_v: bfloat16 [8, 16384, 2048], P('dp', 'sp')
- grad_w_out: float32 [2048, 2048], P('dp')
- grad_w_mix: float32 [16, 128, 128], replicated
- grad_mix_bias: float32 [16, 128], replicated
- grad_gain: float32 [16, 128], replicated
- grad_shift: float32 [16, 128], replicated
All inputs are finite; a program needn't handle non-finite values.
Results may differ from a plain program's by a relative error of at most 0.012.
Values may be sent and summed in bfloat16 or wider, within the bound.
A program may use at most 192 MiB of HBM per device.

v0:
```python
import jax
import jax.numpy as jnp
from jax import lax
from jax.sharding import PartitionSpec as P

EPS = 1e-05


def together(arrays, axis):
    ends = [0]
    for a in arrays:
        ends.append(ends[-1] + a.size)
    total = lax.psum(jnp.concatenate([a.ravel() for a in arrays]), axis)
    return tuple((total[b:e].reshape(a.shape) for a, b, e in zip(arrays, ends, ends[1:])))


def mechanism(grad_s, u_pre, v_pre, w_mix, mix_bias, gain, shift):
    items, length, width = grad_s.shape
    groups, span = (w_mix.shape[0], w_mix.shape[1])
    chans = width // groups
    shape = (items, length // span, span, groups, chans)
    u_val = u_pre.astype(jnp.float32).reshape(shape)
    v_val = v_pre.astype(jnp.float32).reshape(shape)
    cotan = grad_s.astype(jnp.float32).reshape(shape)
    upper, u_back = jax.vjp(jax.nn.gelu, u_val)
    gated, v_back = jax.vjp(jax.nn.gelu, v_val)
    centre = gated - jnp.mean(gated, axis=-1, keepdims=True)
    inverse = lax.rsqrt(jnp.mean(centre * centre, axis=-1, keepdims=True) + EPS)
    scaled = centre * inverse
    normed = (scaled * gain + shift).astype(jnp.bfloat16)
    lower = jnp.tril(jnp.ones((span, span), dtype=bool))
    w_low = jnp.where(lower[None], w_mix, jnp.zeros_like(w_mix))
    mixed = jnp.einsum("gts,insgc->intgc", w_low, normed, preferred_element_type=jnp.float32)
    mixed = mixed + jnp.transpose(mix_bias)[:, :, None]
    gated_out = (upper * mixed).astype(jnp.bfloat16)
    d_mixed = cotan * upper
    d_mixed_b = d_mixed.astype(jnp.bfloat16)
    grad_u = u_back(cotan * mixed)[0].astype(jnp.bfloat16).reshape(items, length, width)
    grad_bias = jnp.transpose(jnp.sum(d_mixed, axis=(0, 1, 4)))
    grad_w = jnp.einsum("intgc,insgc->gts", d_mixed_b, normed, preferred_element_type=jnp.float32)
    grad_w = jnp.where(lower[None], grad_w, jnp.zeros_like(grad_w))
    d_normed = jnp.einsum("gts,intgc->insgc", w_low, d_mixed_b, preferred_element_type=jnp.float32)
    grad_gain = jnp.sum(d_normed * scaled, axis=(0, 1, 2))
    grad_shift = jnp.sum(d_normed, axis=(0, 1, 2))
    d_scaled = d_normed * gain
    d_gated = inverse * (
        d_scaled
        - jnp.mean(d_scaled, axis=-1, keepdims=True)
        - scaled * jnp.mean(d_scaled * scaled, axis=-1, keepdims=True)
    )
    grad_v = v_back(d_gated)[0].astype(jnp.bfloat16).reshape(items, length, width)
    return (
        grad_u,
        grad_v,
        gated_out.reshape(items, length, width),
        grad_w,
        grad_bias,
        grad_gain,
        grad_shift,
    )


def on_device(u_pre, v_pre, d_out, w_mix, mix_bias, norm_gain, norm_shift, w_out):
    grad_s = lax.dot_general(
        d_out,
        lax.all_gather(w_out, "dp", axis=0, tiled=True),
        (((2,), (1,)), ((), ())),
        preferred_element_type=jnp.float32,
    ).astype(jnp.bfloat16)
    grad_u, grad_v, gated_out, grad_w, grad_bias, grad_gain, grad_shift = mechanism(
        grad_s, u_pre, v_pre, w_mix, mix_bias, norm_gain, norm_shift
    )
    grad_w, grad_bias, grad_gain, grad_shift = together(
        (grad_w, grad_bias, grad_gain, grad_shift), ("sp", "dp")
    )
    width = gated_out.shape[2]
    flat_d = d_out.reshape(-1, d_out.shape[2])
    flat_s = gated_out.reshape(-1, width)
    partial_rows = lax.psum_scatter(
        lax.dot_general(
            flat_s, flat_d, (((0,), (0,)), ((), ())), preferred_element_type=jnp.float32
        ),
        "dp",
        scatter_dimension=0,
        tiled=True,
    )
    grad_w_out = lax.psum(partial_rows, "sp")
    return (grad_u, grad_v, grad_w_out, grad_w, grad_bias, grad_gain, grad_shift)


def solution(mesh):
    return jax.shard_map(
        on_device,
        mesh=mesh,
        in_specs=(
            P("dp", "sp", None),
            P("dp", "sp", None),
            P("dp", "sp", None),
            P(),
            P(),
            P(),
            P(),
            P("dp", None),
        ),
        out_specs=(P("dp", "sp", None), P("dp", "sp", None), P("dp", None), P(), P(), P(), P()),
        check_vma=False,
    )
```

profile of v0, /device:TPU:0, one launch (start us, length us, event | category | flops | bytes accessed | tf_op | source)
XLA Modules:
  0.0 474.1 jit_solution(16673040196392679940)
XLA Ops:
  7.2 0.0 all-gather.2.cloned.1.call-start
  7.2 0.7 all-gather.2.cloned.1.call-update
  7.9 0.0 reduce-scatter.2.cloned.1.call-start
  7.9 3.2 convert_bitcast_fusion
  11.2 5.2 %copy.67 = f32[128,8,16,128]{3,2,1,0:T(8,128)} copy(f32[128,8,16,128]{3,1,2,0:T(8,128)S(1)} %convert_bitcast_fusion) | data formatting | bytes 16777216
  16.4 9.1 %copy.45 = f32[1,8,128,16,128]{2,4,1,3,0:T(8,128)} copy(f32[1,8,128,16,128]{4,3,0,2,1:T(8,128)} %bitcast.100) | data formatting | bytes 16777216 | tf_op jit(solution)/shard_map/reshape | solution.py:22
  25.5 3.2 convert_bitcast_fusion.1
  28.8 5.2 %copy.65 = f32[128,8,16,128]{3,2,1,0:T(8,128)} copy(f32[128,8,16,128]{3,1,2,0:T(8,128)S(1)} %convert_bitcast_fusion.1) | data formatting | bytes 16777216
  34.0 8.7 %copy.39 = f32[1,8,128,16,128]{2,4,1,3,0:T(8,128)} copy(f32[1,8,128,16,128]{4,3,0,2,1:T(8,128)} %bitcast.104) | data formatting | bytes 16777216 | tf_op jit(solution)/shard_map/reshape | solution.py:23
  42.7 0.0 copy-start.1
  42.7 0.0 copy-start.3
  42.7 0.0 copy-start.4
  42.8 5.9 %fusion.54 = f32[8,128,16]{1,0,2:T(8,128)S(1)} fusion(f32[1,8,128,16,128]{2,4,1,3,0:T(8,128)} %copy.39), kind=kLoop, calls=%fused_computation.83 | loop fusion | flops 18857984 | bytes 8454144 | tf_op jit(solution)/shard_map/reduce_sum | solution.py:27
  48.6 0.2 copy-done
  48.9 3.7 multiply_reduce_fusion.2
  52.6 0.0 copy-done.1
  52.6 0.0 copy-done.3
  52.7 0.0 copy-done.4
  52.7 6.5 %fusion.35 = bf16[8,128,16,128]{3,1,0,2:T(8,128)(2,1)} fusion(f32[8,128,16,128]{3,2,1,0:T(8,128)S(1)} %bitcast.105, f32[16,128]{1,0:T(8,128)S(1)} %copy-done.4, f32[16,128]{1,0:T(8,128)S(1)} %copy-done.3, f32[8,128,16]{1,0,2:T(8,128)S(1)} %add_rsqrt_fusion, f32[8,128,16]{1,0,2:T(8,128)S(1)} %broadcast_multiply_fusion.2), kind=kLoop, calls=%fused_computation.52 | loop fusion | flops 27262976 | bytes 12730368 | tf_op jit(solution)/shard_map/convert_element_type | solution.py:30
  59.1 2.7 all-gather.2.cloned.1.call-done
  61.8 13.1 %convert_bitcast_fusion.2 = f32[128,8,16,128]{3,1,2,0:T(8,128)S(1)} fusion(bf16[2048,2048]{1,0:T(8,128)(2,1)} %all-gather.2.cloned.1.call-done, bf16[1,1024,2048]{2,1,0:T(8,128)(2,1)} %param.10), kind=kOutput, calls=%fused_computation.51 | convolution fusion | flops 8594128896 | bytes 20971520 | tf_op jit(solution)/shard_map/dot_general | solution.py:64
  74.9 5.2 %copy.64 = f32[128,8,16,128]{3,2,1,0:T(8,128)} copy(f32[128,8,16,128]{3,1,2,0:T(8,128)S(1)} %convert_bitcast_fusion.2) | data formatting | bytes 16777216
  80.1 8.8 %copy.41 = f32[1,8,128,16,128]{2,4,1,3,0:T(8,128)} copy(f32[1,8,128,16,128]{4,3,2,1,0:T(8,128)} %bitcast.102) | data formatting | bytes 16777216 | tf_op jit(solution)/shard_map/reshape | solution.py:24
  88.9 0.0 copy-done.5
  88.9 14.8 %multiply_convert_fusion = (bf16[1,8,128,16,128]{2,4,1,3,0:T(8,128)(2,1)}, bf16[1,8,128,16,128]{2,4,1,3,0:T(8,128)(2,1)}, f32[128,16]{0,1:T(8,128)S(1)}) fusion(f32[128,16]{0,1:T(8,128)S(1)} %bitcast.112, f32[1,8,128,16,128]{2,4,1,3,0:T(8,128)} %copy.45, f32[1,8,128,16,128]{2,4,1,3,0:T(8,128)} %copy.41, bf16[8,128,16,128]{3,1,0,2:T(8,128)(2,1)} %fusion.35, ...), kind=kOutput, calls=%fused_computation.46 | convolution fusion | flops 593754112 | bytes 29917184 | tf_op jit(solution)/shard_map/gts,insgc->intgc/dot_general | solution.py:33
  103.7 6.8 %copy.58 = bf16[1,8,128,16,128]{4,3,2,1,0:T(8,128)(2,1)} copy(bf16[1,8,128,16,128]{2,4,1,3,0:T(8,128)(2,1)} %get-tuple-element.11) | data formatting | bytes 8388608 | tf_op jit(solution)/shard_map/convert_element_type | solution.py:35
  110.5 15.4 %fusion.37 = f32[2048,2048]{1,0:T(8,128)} fusion(bf16[128,8,16,128]{3,2,1,0:T(8,128)(2,1)} %bitcast.107, bf16[1,1024,2048]{2,1,0:T(8,128)(2,1)} %param.10), kind=kOutput, calls=%fused_computation.57 | convolution fusion | flops 8589934592 | bytes 25165824 | tf_op jit(solution)/shard_map/dot_general | solution.py:80
  125.9 0.0 reduce-scatter.2.cloned.1.call-update
  125.9 0.0 all-reduce.5.cloned.1.call-start
  125.9 0.0 copy-start.2
  125.9 10.2 %fusion.33 = bf16[8,128,16,128]{3,1,0,2:T(8,128)(2,1)S(1)} fusion(f32[8,128,16,128]{3,2,1,0:T(8,128)} %bitcast.103, f32[8,128,16,128]{3,2,1,0:T(8,128)} %bitcast.101), kind=kLoop, calls=%fused_computation.39 | loop fusion | flops 20971520 | bytes 20971520 | tf_op jit(solution)/shard_map/convert_element_type | solution.py:37
  136.2 1.3 fusion.45
  137.4 10.3 %fusion.34 = (f32[16,128]{1,0:T(8,128)S(1)}, f32[8,128,16]{1,0,2:T(8,128)S(1)}, f32[8,128,16]{1,0,2:T(8,128)S(1)}, f32[16,128]{1,0:T(8,128)S(1)}, f32[16,8,128,128]{3,2,1,0:T(8,128)}) fusion(f32[8,128,16]{1,0,2:T(8,128)S(1)} %add_rsqrt_fusion, f32[8,128,16]{1,0,2:T(8,128)S(1)} %broadcast_multiply_fusion.2, f32[1,8,128,16,128]{2,4,1,3,0:T(8,128)} %copy.39, ...), kind=kOutput, calls=%fused_computation.44 | convolution fusion | flops 572747776 | bytes 21798912 | tf_op jit(solution)/shard_map/gts,intgc->insgc/dot_general | solution.py:42
  147.7 1.0 pad_maximum_fusion
  148.8 0.0 all-reduce.5.cloned.1.call-update
  148.8 0.0 all-reduce.3.cloned.1.call-start
  148.9 7.0 %copy.47 = bf16[1,8,128,16,128]{4,3,2,1,0:T(8,128)(2,1)} copy(bf16[1,8,128,16,128]{2,4,1,3,0:T(8,128)(2,1)} %get-tuple-element.12) | data formatting | bytes 8388608 | tf_op jit(solution)/shard_map/convert_element_type | solution.py:38
  155.8 7.3 %reshape.497 = bf16[1,1024,2048]{2,1,0:T(8,128)(2,1)} reshape(bf16[1,8,128,16,128]{4,3,2,1,0:T(8,128)(2,1)} %copy.47) | data formatting | bytes 8388608 | tf_op jit(solution)/shard_map/reshape | solution.py:38
  163.2 54.8 %reduce-scatter.2.cloned.1.call-done = f32[256,2048]{1,0:T(8,128)} async-done(((f32[2048,2048]{1,0:T(8,128)}), f32[256,2048]{1,0:T(8,128)}) %reduce-scatter.2.cloned.1.call-update) | async-done | bytes 2097168 | tf_op jit(solution)/shard_map/reduce_scatter | solution.py:79
  217.9 0.0 all-reduce.3.cloned.1.call-update
  218.0 12.0 %fusion.6 = bf16[1,8,128,16,128]{2,4,1,3,0:T(8,128)(2,1)} fusion(f32[1,8,128,16,128]{2,4,1,3,0:T(8,128)} %copy.39, f32[16,8,128,128]{3,2,1,0:T(8,128)} %get-tuple-element.17, f32[8,128,16]{1,0,2:T(8,128)S(1)} %get-tuple-element.18, f32[8,128,16]{1,0,2:T(8,128)S(1)} %get-tuple-element.19, f32[16,128]{1,0:T(8,128)S(1)} %copy-done.3, ...), kind=kLoop, calls=%fused_computation.12 | loop fusion | flops 58720256 | bytes 21241856 | tf_op jit(solution)/shard_map/convert_element_type | solution.py:51
  230.0 6.7 %copy.56 = bf16[1,8,128,16,128]{4,3,2,1,0:T(8,128)(2,1)} copy(bf16[1,8,128,16,128]{2,4,1,3,0:T(8,128)(2,1)} %fusion.6) | data formatting | bytes 8388608 | tf_op jit(solution)/shard_map/convert_element_type | solution.py:51
  236.8 7.3 %reshape.500 = bf16[1,1024,2048]{2,1,0:T(8,128)(2,1)} reshape(bf16[1,8,128,16,128]{4,3,2,1,0:T(8,128)(2,1)} %copy.56) | data formatting | bytes 8388608 | tf_op jit(solution)/shard_map/reshape | solution.py:51
  244.1 127.2 %all-reduce.5.cloned.1.call-done = f32[268288]{0:T(1024)} async-done(((f32[268288]{0:T(1024)}), f32[268288]{0:T(1024)}) %all-reduce.5.cloned.1.call-update) | async-done | bytes 1073168 | tf_op jit(solution)/shard_map/psum | solution.py:13
  371.2 2.3 slice.49
  373.5 1.3 slice_bitcast_fusion
  374.8 89.4 %all-reduce.3.cloned.1.call-done = f32[256,2048]{1,0:T(8,128)} async-done(((f32[256,2048]{1,0:T(8,128)}), f32[256,2048]{1,0:T(8,128)}) %all-reduce.3.cloned.1.call-update) | async-done | bytes 2097168 | tf_op jit(solution)/shard_map/psum | solution.py:87
  464.2 3.1 copy.82
  (9 shorter events, 0.1 us)
Async XLA Ops:
  7.2 54.7 %all-gather.2.cloned.1.call-start = ((), (), s32[]{:S(2)}) async-start(), calls=%async_computation.1 | async-start | bytes 9437184 | tf_op jit(solution)/shard_map/all_gather | solution.py:66
  7.9 210.1 %reduce-scatter.2.cloned.1.call-start = ((), (), s32[]{:S(2)}) async-start(), calls=%async_computation.2 | async-start | bytes 18874368 | tf_op jit(solution)/shard_map/reduce_scatter | solution.py:79
  42.7 6.2 %copy-start = (f32[1,8,128,16,128]{2,4,1,3,0:T(8,128)S(1)}, f32[1,8,128,16,128]{2,4,1,3,0:T(8,128)}, u32[]{:S(2)}) copy-start(f32[1,8,128,16,128]{2,4,1,3,0:T(8,128)} %copy.39) | copy-start | bytes 25165828
  42.7 9.9 %copy-start.1 = (f32[128,8,16,128]{3,2,1,0:T(8,128)S(1)}, f32[128,8,16,128]{3,2,1,0:T(8,128)}, u32[]{:S(2)}) copy-start(f32[128,8,16,128]{3,2,1,0:T(8,128)} %copy.65) | copy-start | bytes 25165828
  42.7 9.9 %copy-start.3 = (f32[16,128]{1,0:T(8,128)S(1)}, f32[16,128]{1,0:T(8,128)}, u32[]{:S(2)}) copy-start(f32[16,128]{1,0:T(8,128)} %param.13) | copy-start | bytes 24580
  42.7 9.9 %copy-start.4 = (f32[16,128]{1,0:T(8,128)S(1)}, f32[16,128]{1,0:T(8,128)}, u32[]{:S(2)}) copy-start(f32[16,128]{1,0:T(8,128)} %param.14) | copy-start | bytes 24580
  80.1 8.8 %copy-start.5 = (bf16[16,128,128]{2,1,0:T(8,128)(2,1)S(1)}, bf16[16,128,128]{2,1,0:T(8,128)(2,1)}, u32[]{:S(2)}) copy-start(bf16[16,128,128]{2,1,0:T(8,128)(2,1)} %param.11) | copy-start | bytes 1572868
  80.1 8.8 %copy-start.6 = (f32[16,128]{1,0:T(8,128)S(1)}, f32[16,128]{1,0:T(8,128)}, u32[]{:S(2)}) copy-start(f32[16,128]{1,0:T(8,128)} %param.12) | copy-start | bytes 24580
  125.9 245.4 %all-reduce.5.cloned.1.call-start = ((), (), s32[]{:S(2)}) async-start(), calls=%async_computation.4 | async-start | bytes 2146304 | tf_op jit(solution)/shard_map/psum | solution.py:13
  125.9 10.2 %copy-start.2 = (bf16[8,128,16,128]{3,1,0,2:T(8,128)(2,1)S(1)}, bf16[8,128,16,128]{3,1,0,2:T(8,128)(2,1)}, u32[]{:S(2)}) copy-start(bf16[8,128,16,128]{3,1,0,2:T(8,128)(2,1)} %fusion.35) | copy-start | bytes 12582916
  148.8 315.4 %all-reduce.3.cloned.1.call-start = ((), (), s32[]{:S(2)}) async-start(), calls=%async_computation.3 | async-start | bytes 4194304 | tf_op jit(solution)/shard_map/psum | solution.py:87
Sparse Core Ops, SparseCore 0:
  9.7 52.0 all-gather.1
  126.0 91.9 reduce-scatter.1
  223.3 147.8 all-reduce.4
  374.4 89.7 all-reduce.2
where the time goes:
time: 478 us; the launch traced here: 474 us
  waiting for transfers between devices  275 us (58%)
  local copies, waits for them, and re-layouts  84.4 us (18%)
  matrix products  54.8 us (11%)
  other arithmetic  45.8 us (10%)
  between operations  14.1 us (3%)
    psum x1, waiting for transfers between devices, together(): total = lax.psum(jnp.concatenate([a.ravel() for a in arrays]), axis)  127 us
    psum x1, waiting for transfers between devices, on_device(): grad_w_out = lax.psum(partial_rows, 'sp')  89.4 us
    reduce_scatter x1, waiting for transfers between devices, on_device(): lax.psum_scatter(lax.dot_general(flat_s, flat_d, (((0,), (0,)), ((), ()))...  54.8 us
    unnamed x18, local copies, waits for them, and re-layouts  19 us
    dot_general x1, matrix products, on_device(): lax.dot_general(flat_s, flat_d, (((0,), (0,)), ((), ())), preferred_eleme...  15.4 us
    dot_general x1, matrix products, mechanism(): jnp.einsum('gts,insgc->intgc', w_low, normed, preferred_element_type=jnp....  14.8 us
    dot_general x1, matrix products, on_device(): lax.dot_general(d_out, lax.all_gather(w_out, 'dp', axis=0, tiled=True), (...  13.1 us
    convert_element_type x1, other arithmetic, mechanism(): v_back(d_gated)[0].astype(jnp.bfloat16).reshape(items, length, width)  12 us
  transfers between devices with their start and end apart: 4, of which 4 were waited for; matrix products, arithmetic and copies ran while one was open for 25% of the time, Pallas kernels for 0%

commit v1 on v0

--- a/solution.py
+++ b/solution.py
@@ -84,7 +84,11 @@
         scatter_dimension=0,
         tiled=True,
     )
-    grad_w_out = lax.psum(partial_rows, "sp")
+    grad_w_out = partial_rows
+    for hop in (1, 2, 4, 8):
+        grad_w_out = grad_w_out + lax.ppermute(
+            grad_w_out, "sp", [(dev, dev ^ hop) for dev in range(16)]
+        )
     return (grad_u, grad_v, grad_w_out, grad_w, grad_bias, grad_gain, grad_shift)
 
 

time: 478 us -> 528 us (1.10)
  waiting for transfers between devices: 275 us -> 312 us
  starting transfers between devices: 0.16 us -> 9.64 us
  other arithmetic: 45.8 us -> 54.1 us
    ppermute x0 -> x4, waiting for transfers between devices: none -> 115 us  [on_device(): lax.ppermute(grad_w_out, 'sp', [(dev, dev ^ hop) for dev in range(16)])]
    psum x1 -> x0, waiting for transfers between devices: 89.4 us -> none  [on_device(): grad_w_out = lax.psum(partial_rows, 'sp')]
    reduce_scatter x1, waiting for transfers between devices: 54.8 us -> 92 us  [on_device(): lax.psum_scatter(lax.dot_general(flat_s, flat_d, (((0,), (0,)), ((), ()))...]
    psum x1, waiting for transfers between devices: 127 us -> 102 us  [together(): total = lax.psum(jnp.concatenate([a.ravel() for a in arrays]), axis)]
    ppermute x0 -> x4, starting transfers between devices: none -> 9.52 us  [on_device(): lax.ppermute(grad_w_out, 'sp', [(dev, dev ^ hop) for dev in range(16)])]
    add x0 -> x4, other arithmetic: none -> 7.96 us  [on_device(): grad_w_out + lax.ppermute(grad_w_out, 'sp', [(dev, dev ^ hop) for dev in...]
    unnamed x18 -> x23, local copies, waits for them, and re-layouts: 19 us -> 15.8 us
  transfers between devices with their start and end apart: 4 -> 7, of which waited for: 4 -> 6; matrix products, arithmetic and copies ran while one was open for 25% -> 22% of each run, Pallas kernels for 0% -> 0%
where the time goes in v1:
time: 528 us; the launch traced here: 523 us
  waiting for transfers between devices  312 us (59%)
  local copies, waits for them, and re-layouts  80.8 us (15%)
  other arithmetic  54.1 us (10%)
  matrix products  52.5 us (10%)
  between operations  14.2 us (3%)
  starting transfers between devices  9.64 us (2%)
    ppermute x4, waiting for transfers between devices, on_device(): lax.ppermute(grad_w_out, 'sp', [(dev, dev ^ hop) for dev in range(16)])  115 us
    psum x1, waiting for transfers between devices, together(): total = lax.psum(jnp.concatenate([a.ravel() for a in arrays]), axis)  102 us
    reduce_scatter x1, waiting for transfers between devices, on_device(): lax.psum_scatter(lax.dot_general(flat_s, flat_d, (((0,), (0,)), ((), ()))...  92 us
    unnamed x23, local copies, waits for them, and re-layouts  15.8 us
    dot_general x1, matrix products, on_device(): lax.dot_general(flat_s, flat_d, (((0,), (0,)), ((), ())), preferred_eleme...  15.4 us
    dot_general x1, matrix products, mechanism(): jnp.einsum('gts,insgc->intgc', w_low, normed, preferred_element_type=jnp....  14.8 us
    dot_general x1, matrix products, on_device(): lax.dot_general(d_out, lax.all_gather(w_out, 'dp', axis=0, tiled=True), (...  13.1 us
    convert_element_type x1, other arithmetic, mechanism(): v_back(d_gated)[0].astype(jnp.bfloat16).reshape(items, length, width)  12.2 us
  transfers between devices with their start and end apart: 7, of which 6 were waited for; matrix products, arithmetic and copies ran while one was open for 22% of the time, Pallas kernels for 0%

profile of v1, /device:TPU:0, one launch (start us, length us, event | category | flops | bytes accessed | tf_op | source)
XLA Modules:
  0.0 523.4 jit_solution(356376718351816498)
XLA Ops:
  7.2 0.0 all-gather.2.cloned.1.call-start
  7.2 0.7 all-gather.2.cloned.1.call-update
  7.9 0.0 reduce-scatter.2.cloned.1.call-start
  7.9 3.2 convert_bitcast_fusion
  11.2 5.2 copy.67
  16.4 9.1 %copy.45 = f32[1,8,128,16,128]{2,4,1,3,0:T(8,128)} copy(f32[1,8,128,16,128]{4,3,0,2,1:T(8,128)} %bitcast.102) | data formatting | bytes 16777216 | tf_op jit(solution)/shard_map/reshape | solution.py:22
  25.5 3.2 convert_bitcast_fusion.1
  28.7 5.2 copy.65
  33.9 8.7 %copy.39 = f32[1,8,128,16,128]{2,4,1,3,0:T(8,128)} copy(f32[1,8,128,16,128]{4,3,0,2,1:T(8,128)} %bitcast.106) | data formatting | bytes 16777216 | tf_op jit(solution)/shard_map/reshape | solution.py:23
  42.7 0.0 copy-start.4
  42.7 5.9 %fusion.54 = f32[8,128,16]{1,0,2:T(8,128)S(1)} fusion(f32[1,8,128,16,128]{2,4,1,3,0:T(8,128)} %copy.39), kind=kLoop, calls=%fused_computation.83 | loop fusion | flops 18857984 | bytes 8454144 | tf_op jit(solution)/shard_map/reduce_sum | solution.py:27
  48.6 0.2 copy-done
  48.8 3.7 multiply_reduce_fusion.2
  52.6 6.5 %fusion.35 = bf16[8,128,16,128]{3,1,0,2:T(8,128)(2,1)} fusion(f32[8,128,16,128]{3,2,1,0:T(8,128)S(1)} %bitcast.107, f32[16,128]{1,0:T(8,128)S(1)} %copy-done.5, f32[16,128]{1,0:T(8,128)S(1)} %copy-done.4, f32[8,128,16]{1,0,2:T(8,128)S(1)} %add_rsqrt_fusion, f32[8,128,16]{1,0,2:T(8,128)S(1)} %broadcast_multiply_fusion.2), kind=kLoop, calls=%fused_computation.52 | loop fusion | flops 27262976 | bytes 12730368 | tf_op jit(solution)/shard_map/convert_element_type | solution.py:30
  59.1 2.7 all-gather.2.cloned.1.call-done
  61.8 13.1 %convert_bitcast_fusion.2 = f32[128,8,16,128]{3,1,2,0:T(8,128)S(1)} fusion(bf16[2048,2048]{1,0:T(8,128)(2,1)} %all-gather.2.cloned.1.call-done, bf16[1,1024,2048]{2,1,0:T(8,128)(2,1)} %param.10), kind=kOutput, calls=%fused_computation.51 | convolution fusion | flops 8594128896 | bytes 20971520 | tf_op jit(solution)/shard_map/dot_general | solution.py:64
  74.9 5.2 copy.64
  80.1 8.8 %copy.41 = f32[1,8,128,16,128]{2,4,1,3,0:T(8,128)} copy(f32[1,8,128,16,128]{4,3,2,1,0:T(8,128)} %bitcast.104) | data formatting | bytes 16777216 | tf_op jit(solution)/shard_map/reshape | solution.py:24
  88.9 14.8 %multiply_convert_fusion = (bf16[1,8,128,16,128]{2,4,1,3,0:T(8,128)(2,1)}, bf16[1,8,128,16,128]{2,4,1,3,0:T(8,128)(2,1)}, f32[128,16]{0,1:T(8,128)S(1)}) fusion(f32[128,16]{0,1:T(8,128)S(1)} %bitcast.114, f32[1,8,128,16,128]{2,4,1,3,0:T(8,128)} %copy.45, f32[1,8,128,16,128]{2,4,1,3,0:T(8,128)} %copy.41, bf16[8,128,16,128]{3,1,0,2:T(8,128)(2,1)} %fusion.35, ...), kind=kOutput, calls=%fused_computation.46 | convolution fusion | flops 593754112 | bytes 29917184 | tf_op jit(solution)/shard_map/gts,insgc->intgc/dot_general | solution.py:33
  103.7 6.8 %copy.58 = bf16[1,8,128,16,128]{4,3,2,1,0:T(8,128)(2,1)} copy(bf16[1,8,128,16,128]{2,4,1,3,0:T(8,128)(2,1)} %get-tuple-element.11) | data formatting | bytes 8388608 | tf_op jit(solution)/shard_map/convert_element_type | solution.py:35
  110.5 15.4 %fusion.37 = f32[2048,2048]{1,0:T(8,128)} fusion(bf16[128,8,16,128]{3,2,1,0:T(8,128)(2,1)} %bitcast.109, bf16[1,1024,2048]{2,1,0:T(8,128)(2,1)} %param.10), kind=kOutput, calls=%fused_computation.57 | convolution fusion | flops 8589934592 | bytes 25165824 | tf_op jit(solution)/shard_map/dot_general | solution.py:80
  125.9 0.0 reduce-scatter.2.cloned.1.call-update
  125.9 0.0 all-reduce.2.cloned.1.call-start
  125.9 92.0 %reduce-scatter.2.cloned.1.call-done = f32[256,2048]{1,0:T(8,128)} async-done(((f32[2048,2048]{1,0:T(8,128)}), f32[256,2048]{1,0:T(8,128)}) %reduce-scatter.2.cloned.1.call-update) | async-done | bytes 2097168 | tf_op jit(solution)/shard_map/reduce_scatter | solution.py:79
  218.0 1.5 collective-permute-start
  219.5 45.6 %collective-permute-done = f32[256,2048]{1,0:T(8,128)S(1)} collective-permute-done((f32[256,2048]{1,0:T(8,128)}, f32[256,2048]{1,0:T(8,128)S(1)}, u32[]{:S(2)}, u32[]{:S(2)}) %collective-permute-start) | collective-permute-done | bytes 2097184 | tf_op jit(solution)/shard_map/ppermute | solution.py:89
  265.0 2.0 add.205
  267.0 3.1 collective-permute-start.1
  270.1 10.2 %fusion.33 = bf16[8,128,16,128]{3,1,0,2:T(8,128)(2,1)S(1)} fusion(f32[8,128,16,128]{3,2,1,0:T(8,128)} %bitcast.105, f32[8,128,16,128]{3,2,1,0:T(8,128)} %bitcast.103), kind=kLoop, calls=%fused_computation.39 | loop fusion | flops 20971520 | bytes 20971520 | tf_op jit(solution)/shard_map/convert_element_type | solution.py:37
  280.4 1.3 fusion.45
  281.7 8.0 %fusion.34 = (f32[16,128]{1,0:T(8,128)S(1)}, f32[8,128,16]{1,0,2:T(8,128)S(1)}, f32[8,128,16]{1,0,2:T(8,128)S(1)}, f32[16,128]{1,0:T(8,128)S(1)}, f32[16,8,128,128]{3,2,1,0:T(8,128)}) fusion(f32[8,128,16]{1,0,2:T(8,128)S(1)} %add_rsqrt_fusion, f32[8,128,16]{1,0,2:T(8,128)S(1)} %broadcast_multiply_fusion.2, f32[1,8,128,16,128]{2,4,1,3,0:T(8,128)S(1)} %bitcast.101, ...), kind=kOutput, calls=%fused_computation.44 | convolution fusion | flops 572747776 | bytes 21798912 | tf_op jit(solution)/shard_map/gts,intgc->insgc/dot_general | solution.py:42
  289.7 25.0 %collective-permute-done.1 = f32[256,2048]{1,0:T(8,128)S(1)} collective-permute-done((f32[256,2048]{1,0:T(8,128)S(1)}, f32[256,2048]{1,0:T(8,128)S(1)}, u32[]{:S(2)}, u32[]{:S(2)}) %collective-permute-start.1) | collective-permute-done | bytes 2097184 | tf_op jit(solution)/shard_map/ppermute | solution.py:89
  314.6 0.3 add.206
  315.0 1.9 collective-permute-start.2
  316.8 1.1 pad_maximum_fusion
  318.0 0.0 all-reduce.2.cloned.1.call-update
  318.0 44.5 %collective-permute-done.2 = f32[256,2048]{1,0:T(8,128)} collective-permute-done((f32[256,2048]{1,0:T(8,128)S(1)}, f32[256,2048]{1,0:T(8,128)}, u32[]{:S(2)}, u32[]{:S(2)}) %collective-permute-start.2) | collective-permute-done | bytes 2097184 | tf_op jit(solution)/shard_map/ppermute | solution.py:89
  362.5 2.5 add.207
  365.0 3.0 collective-permute-start.3
  368.1 12.2 %fusion.6 = bf16[1,8,128,16,128]{2,4,1,3,0:T(8,128)(2,1)} fusion(f32[1,8,128,16,128]{2,4,1,3,0:T(8,128)} %copy.39, f32[16,8,128,128]{3,2,1,0:T(8,128)} %get-tuple-element.17, f32[8,128,16]{1,0,2:T(8,128)S(1)} %get-tuple-element.18, f32[8,128,16]{1,0,2:T(8,128)S(1)} %get-tuple-element.19, f32[16,128]{1,0:T(8,128)S(1)} %copy-done.4, ...), kind=kLoop, calls=%fused_computation.12 | loop fusion | flops 58720256 | bytes 21241856 | tf_op jit(solution)/shard_map/convert_element_type | solution.py:51
  380.3 6.7 %copy.47 = bf16[1,8,128,16,128]{4,3,2,1,0:T(8,128)(2,1)} copy(bf16[1,8,128,16,128]{2,4,1,3,0:T(8,128)(2,1)} %get-tuple-element.12) | data formatting | bytes 8388608 | tf_op jit(solution)/shard_map/convert_element_type | solution.py:38
  387.0 7.3 %reshape.497 = bf16[1,1024,2048]{2,1,0:T(8,128)(2,1)} reshape(bf16[1,8,128,16,128]{4,3,2,1,0:T(8,128)(2,1)} %copy.47) | data formatting | bytes 8388608 | tf_op jit(solution)/shard_map/reshape | solution.py:38
  394.2 6.8 %copy.56 = bf16[1,8,128,16,128]{4,3,2,1,0:T(8,128)(2,1)} copy(bf16[1,8,128,16,128]{2,4,1,3,0:T(8,128)(2,1)} %fusion.6) | data formatting | bytes 8388608 | tf_op jit(solution)/shard_map/convert_element_type | solution.py:51
  401.0 7.3 %reshape.500 = bf16[1,1024,2048]{2,1,0:T(8,128)(2,1)} reshape(bf16[1,8,128,16,128]{4,3,2,1,0:T(8,128)(2,1)} %copy.56) | data formatting | bytes 8388608 | tf_op jit(solution)/shard_map/reshape | solution.py:51
  408.3 101.6 %all-reduce.2.cloned.1.call-done = f32[268288]{0:T(1024)} async-done(((f32[268288]{0:T(1024)}), f32[268288]{0:T(1024)}) %all-reduce.2.cloned.1.call-update) | async-done | bytes 1073168 | tf_op jit(solution)/shard_map/psum | solution.py:13
  509.8 2.3 slice.49
  512.1 1.3 slice_bitcast_fusion
  513.4 3.2 add.208
  (24 shorter events, 0.1 us)
Async XLA Ops:
  7.2 54.7 %all-gather.2.cloned.1.call-start = ((), (), s32[]{:S(2)}) async-start(), calls=%async_computation.1 | async-start | bytes 9437184 | tf_op jit(solution)/shard_map/all_gather | solution.py:66
  7.9 210.1 %reduce-scatter.2.cloned.1.call-start = ((), (), s32[]{:S(2)}) async-start(), calls=%async_computation.2 | async-start | bytes 18874368 | tf_op jit(solution)/shard_map/reduce_scatter | solution.py:79
  42.7 6.2 %copy-start = (f32[1,8,128,16,128]{2,4,1,3,0:T(8,128)S(1)}, f32[1,8,128,16,128]{2,4,1,3,0:T(8,128)}, u32[]{:S(2)}) copy-start(f32[1,8,128,16,128]{2,4,1,3,0:T(8,128)} %copy.39) | copy-start | bytes 25165828
  42.7 9.9 %copy-start.1 = (f32[128,8,16,128]{3,2,1,0:T(8,128)S(1)}, f32[128,8,16,128]{3,2,1,0:T(8,128)}, u32[]{:S(2)}) copy-start(f32[128,8,16,128]{3,2,1,0:T(8,128)} %copy.65) | copy-start | bytes 25165828
  42.7 9.9 %copy-start.4 = (f32[16,128]{1,0:T(8,128)S(1)}, f32[16,128]{1,0:T(8,128)}, u32[]{:S(2)}) copy-start(f32[16,128]{1,0:T(8,128)} %param.13) | copy-start | bytes 24580
  42.7 9.9 %copy-start.5 = (f32[16,128]{1,0:T(8,128)S(1)}, f32[16,128]{1,0:T(8,128)}, u32[]{:S(2)}) copy-start(f32[16,128]{1,0:T(8,128)} %param.14) | copy-start | bytes 24580
  80.1 8.8 %copy-start.6 = (bf16[16,128,128]{2,1,0:T(8,128)(2,1)S(1)}, bf16[16,128,128]{2,1,0:T(8,128)(2,1)}, u32[]{:S(2)}) copy-start(bf16[16,128,128]{2,1,0:T(8,128)(2,1)} %param.11) | copy-start | bytes 1572868
  80.1 8.8 %copy-start.7 = (f32[16,128]{1,0:T(8,128)S(1)}, f32[16,128]{1,0:T(8,128)}, u32[]{:S(2)}) copy-start(f32[16,128]{1,0:T(8,128)} %param.12) | copy-start | bytes 24580
  125.9 383.9 %all-reduce.2.cloned.1.call-start = ((), (), s32[]{:S(2)}) async-start(), calls=%async_computation.3 | async-start | bytes 2146304 | tf_op jit(solution)/shard_map/psum | solution.py:13
  218.0 47.1 %collective-permute-start = (f32[256,2048]{1,0:T(8,128)}, f32[256,2048]{1,0:T(8,128)S(1)}, u32[]{:S(2)}, u32[]{:S(2)}) collective-permute-start(f32[256,2048]{1,0:T(8,128)} %reduce-scatter.2.cloned.1.call-done), channel_id=1, source_target_pairs={{0,8},{8,0},{16,24},{24,16},{32,40},{40,32},{48,56},{56,48},{64,72... | collective-permute-start | bytes 6291464 | tf_op jit(solution)/shard_map/ppermute | solution.py:89
  265.0 16.6 %slice-start = ((s8[8388608]{0:T(1024)(128)(4,1)}), s8[4194304]{0:T(1024)(128)(4,1)S(1)}, s32[]{:S(2)}) async-start(s8[8388608]{0:T(1024)(128)(4,1)} %bitcast.100), calls=%async_computation.4 | async-start | bytes 8388608
  267.0 47.6 %collective-permute-start.1 = (f32[256,2048]{1,0:T(8,128)S(1)}, f32[256,2048]{1,0:T(8,128)S(1)}, u32[]{:S(2)}, u32[]{:S(2)}) collective-permute-start(f32[256,2048]{1,0:T(8,128)S(1)} %add.205), channel_id=1, source_target_pairs={{0,16},{8,24},{16,0},{24,8},{32,48},{40,56},{48,32},{56,40},{64,80... | collective-permute-start | bytes 6291464 | tf_op jit(solution)/shard_map/ppermute | solution.py:89
  270.1 10.2 %copy-start.2 = (bf16[8,128,16,128]{3,1,0,2:T(8,128)(2,1)S(1)}, bf16[8,128,16,128]{3,1,0,2:T(8,128)(2,1)}, u32[]{:S(2)}) copy-start(bf16[8,128,16,128]{3,1,0,2:T(8,128)(2,1)} %fusion.35) | copy-start | bytes 12582916
  270.1 11.5 %slice-start.1 = ((s8[8388608]{0:T(1024)(128)(4,1)}), s8[4194304]{0:T(1024)(128)(4,1)S(1)}, s32[]{:S(2)}) async-start(s8[8388608]{0:T(1024)(128)(4,1)} %bitcast.100), calls=%async_computation.5 | async-start | bytes 8388608
  315.0 3.0 copy-start.3
  315.0 47.6 %collective-permute-start.2 = (f32[256,2048]{1,0:T(8,128)S(1)}, f32[256,2048]{1,0:T(8,128)}, u32[]{:S(2)}, u32[]{:S(2)}) collective-permute-start(f32[256,2048]{1,0:T(8,128)S(1)} %add.206), channel_id=1, source_target_pairs={{0,32},{8,40},{16,48},{24,56},{32,0},{40,8},{48,16},{56,24},{64,96... | collective-permute-start | bytes 6291464 | tf_op jit(solution)/shard_map/ppermute | solution.py:89
  365.0 148.4 %collective-permute-start.3 = (f32[256,2048]{1,0:T(8,128)S(1)}, f32[256,2048]{1,0:T(8,128)}, u32[]{:S(2)}, u32[]{:S(2)}) collective-permute-start(f32[256,2048]{1,0:T(8,128)S(1)} %add.207), channel_id=1, source_target_pairs={{0,64},{8,72},{16,80},{24,88},{32,96},{40,104},{48,112},{56,120},{... | collective-permute-start | bytes 6291464 | tf_op jit(solution)/shard_map/ppermute | solution.py:89
Sparse Core Ops, SparseCore 0:
  9.7 52.0 all-gather.1
  126.0 91.9 reduce-scatter.1
  318.1 191.6 all-reduce.1
